TPU v7x, 32 devices: a whole 2x2x4 slice. The times are simulated.
32 devices in a mesh: sp: 8 (over z, y), tp: 4 (over x, core).
Axes of the slice: x: 2, y: 2, z: 4, core: 2. Of those that a mesh axis runs over, the one named last changes fastest.
Arguments:
- activations: bfloat16 [4096, 2048], P('sp', 'tp'), may hold values from -250 to 250
- norm_gain: bfloat16 [2048], P('tp'), may hold values from 0.099609375 to 1.8984375
- pool_weight: bfloat16 [2048, 1024], P('sp', 'tp'), may hold values from -0.125 to 0.125
- gate_weight: bfloat16 [2048, 1024], P('sp', 'tp'), may hold values from -0.125 to 0.125
- value_weight: bfloat16 [2048, 1024], P('sp', 'tp'), may hold values from -0.125 to 0.125
- key_weight: bfloat16 [2048, 256], P('sp', 'tp'), may hold values from -0.125 to 0.125
- read_weight: bfloat16 [2048, 256], P('sp', 'tp'), may hold values from -0.125 to 0.125
- step_weight: bfloat16 [2048, 16], P('sp', 'tp'), may hold values from -0.125 to 0.125
- pool_mix: bfloat16 [4, 256, 256], P('tp'), may hold values from -0.375 to 0.375
- pool_scale: float32 [1024], P('tp'), may hold values from 0.1 to 1.9
- taps_value: float32 [4, 1024], P(None, 'tp'), may hold values from -3 to 3
- taps_key: float32 [4, 256], P(None, 'tp'), may hold values from -3 to 3
- taps_read: float32 [4, 256], P(None, 'tp'), may hold values from -3 to 3
- step_bias: float32 [16], P('tp'), may hold values from -1 to 1
- decay_log: float32 [16], P('tp')
- decay_extra: float32 [4096, 16], P('sp', 'tp'), may hold values from -1 to 0
- skip_scale: float32 [16], P('tp'), may hold values from 0.5 to 2
- state_gain: float32 [1024], P('tp'), may hold values from 0.1 to 1.9
- out_pool_weight: bfloat16 [1024, 2048], P('tp', 'sp'), may hold values from -0.125 to 0.125
- out_state_weight: bfloat16 [1024, 2048], P('tp', 'sp'), may hold values from -0.125 to 0.125
Outputs:
- mixed: bfloat16 [4096, 2048], P('sp', 'tp')
All inputs are finite; a program needn't handle non-finite values.
Results may differ from a plain program's by a relative error of at most 0.007.
Values may be sent and summed in bfloat16 or wider, within the bound.
A program may use at most 64 MiB of HBM per device.

v0:
```python
import jax
import jax.numpy as jnp
from jax import lax
from jax.sharding import PartitionSpec as P

SSM_STATE = 64
POOL_GROUPS = 4
SCAN_BLOCK = 128
MIX_W = 1024
EPSILON = 1e-06
HIGH = lax.Precision.HIGHEST


def shifted(value, axis, steps):
    count = lax.axis_size(axis)
    leading, last = (max(0, -steps), min(count, count - steps))
    return lax.ppermute(value, axis, [(source, source + steps) for source in range(leading, last)])


def carried_in(part, axis, combine, identity):
    place = lax.axis_index(axis)
    gathered = jax.tree.map(lambda a: lax.all_gather(a, axis), part)
    state = jax.tree.map(lambda a, e: jnp.zeros_like(a) + jnp.asarray(e, a.dtype), part, identity)

    def one(step, state):
        return combine(
            state, jax.tree.map(lambda a: lax.dynamic_index_in_dim(a, step, 0, False), gathered)
        )

    return lax.fori_loop(0, place, one, state)


def backward_kernel(extended, taps):
    width = taps.shape[0]
    length = extended.shape[0] - (width - 1)
    widened_rows = extended.astype(jnp.float32)
    total = jnp.zeros((length, extended.shape[1]), jnp.float32)
    for offset in range(width):
        total = total + taps[offset][None, :] * widened_rows[offset : offset + length]
    return jax.nn.silu(total).astype(jnp.bfloat16)


def combine_states(preceding_token, later):
    return (preceding_token[0] * later[0], preceding_token[1] * later[0][:, None, None] + later[1])


def local(
    activations,
    norm_gain,
    pool_weight,
    gate_weight,
    value_weight,
    key_weight,
    read_weight,
    step_weight,
    pool_mix,
    pool_scale,
    taps_value,
    taps_key,
    taps_read,
    step_bias,
    decay_log,
    decay_extra,
    skip_scale,
    state_gain,
    out_pool_weight,
    out_state_weight,
):
    length = activations.shape[0]
    cluster_span = pool_weight.shape[1]
    local_mix = gate_weight.shape[1]
    local_state = key_weight.shape[1]
    local_heads = step_weight.shape[1]
    joined = jnp.concatenate(
        [pool_weight, gate_weight, value_weight, key_weight, read_weight, step_weight], axis=1
    )
    in_weight = lax.all_gather(joined, "sp", axis=0, tiled=True)
    whole, gains = (
        lax.all_gather(activations, "tp", axis=1, tiled=True),
        lax.all_gather(norm_gain, "tp", axis=0, tiled=True),
    )
    widened_rows = whole.astype(jnp.float32)
    normed = (
        widened_rows
        * lax.rsqrt(jnp.mean(widened_rows * widened_rows, axis=-1, keepdims=True) + EPSILON)
        * gains.astype(jnp.float32)
    ).astype(jnp.bfloat16)
    projected = jnp.dot(normed, in_weight, preferred_element_type=jnp.float32)
    column = 0
    pool_in = projected[:, column : column + cluster_span].astype(jnp.bfloat16)
    column = column + cluster_span
    gate_in = projected[:, column : column + local_mix].astype(jnp.bfloat16)
    column = column + local_mix
    raw_value = projected[:, column : column + local_mix].astype(jnp.bfloat16)
    column = column + local_mix
    raw_key = projected[:, column : column + local_state].astype(jnp.bfloat16)
    column = column + local_state
    raw_read = projected[:, column : column + local_state].astype(jnp.bfloat16)
    column = column + local_state
    step_raw = projected[:, column : column + local_heads]
    raw_joined = jnp.concatenate([raw_value, raw_key, raw_read], axis=1)
    reach = 2**POOL_GROUPS - 1
    width = taps_value.shape[0]
    prior_pool, prior_joined = shifted(
        (pool_in[length - reach :], raw_joined[length - width + 1 :]), "sp", 1
    )
    group = lax.axis_index("tp")
    running = jnp.concatenate([prior_pool, pool_in], axis=0).astype(jnp.float32)
    levels = []
    for level in range(POOL_GROUPS):
        stride = 2**level
        running = running[stride:] + running[:-stride]
        levels.append(running[running.shape[0] - length :])
    window_sum = lax.dynamic_index_in_dim(jnp.stack(levels), group, 0, keepdims=False)
    window = jnp.exp2((group + 1).astype(jnp.float32))
    position = (lax.axis_index("sp") * length + jnp.arange(length, dtype=jnp.int32)).astype(
        jnp.float32
    )
    counts = jnp.minimum(position + 1.0, window)
    pooled = (window_sum / counts[:, None] - pool_in.astype(jnp.float32)).astype(jnp.bfloat16)
    pool_out = (
        jnp.dot(pooled, pool_mix[0], preferred_element_type=jnp.float32) * pool_scale
    ).astype(jnp.bfloat16)
    all_taps = jnp.concatenate([taps_value, taps_key, taps_read], axis=1)
    convolved = backward_kernel(jnp.concatenate([prior_joined, raw_joined], axis=0), all_taps)
    head_value = convolved[:, :local_mix]
    key_vectors = convolved[:, local_mix : local_mix + local_state]
    read_vectors = convolved[:, local_mix + local_state :]
    head_dim = local_mix // local_heads
    groups_here = local_state // SSM_STATE
    repeat = local_heads // groups_here
    blocks = length // SCAN_BLOCK
    step_size = jax.nn.softplus(step_raw + step_bias)
    log_decay = -jnp.exp(decay_log) * step_size + decay_extra
    value_heads = head_value.astype(jnp.float32).reshape(length, local_heads, head_dim)
    value_blocks = value_heads.reshape(blocks, SCAN_BLOCK, local_heads, head_dim)
    key_blocks = jnp.repeat(
        key_vectors.astype(jnp.float32).reshape(length, groups_here, SSM_STATE), repeat, axis=1
    ).reshape(blocks, SCAN_BLOCK, local_heads, SSM_STATE)
    read_blocks = jnp.repeat(
        read_vectors.astype(jnp.float32).reshape(length, groups_here, SSM_STATE), repeat, axis=1
    ).reshape(blocks, SCAN_BLOCK, local_heads, SSM_STATE)
    step_blocks = step_size.reshape(blocks, SCAN_BLOCK, local_heads)
    running_decay = jnp.cumsum(log_decay.reshape(blocks, SCAN_BLOCK, local_heads), axis=1)
    lower = jnp.arange(SCAN_BLOCK)[:, None] >= jnp.arange(SCAN_BLOCK)[None, :]
    gaps = jnp.where(
        lower[None, :, :, None],
        running_decay[:, :, None, :] - running_decay[:, None, :, :],
        -jnp.inf,
    )
    weights = jnp.einsum("blhn,bshn->blsh", read_blocks, key_blocks, precision=HIGH) * jnp.exp(gaps)
    scaled_value = value_blocks * step_blocks[..., None]
    inner = jnp.einsum("blsh,bshp->blhp", weights, scaled_value, precision=HIGH)
    block_ends = running_decay[:, -1, :]
    trailing = jnp.exp(block_ends[:, None, :] - running_decay)
    fresh = jnp.einsum("bshn,bsh,bshp->bhpn", key_blocks, trailing, scaled_value, precision=HIGH)

    def advance(carry, inputs):
        block_decay, block_state = inputs
        return (carry * block_decay[:, None, None] + block_state, carry)

    local_total, prefix = lax.scan(
        advance,
        jnp.zeros((local_heads, head_dim, SSM_STATE), jnp.float32),
        (jnp.exp(block_ends), fresh),
    )
    offsets = jnp.cumsum(block_ends, axis=0) - block_ends
    device_decay = jnp.exp(offsets[-1] + block_ends[-1])
    incoming_decay, incoming = carried_in(
        (device_decay, local_total),
        "sp",
        combine_states,
        (jnp.ones_like(device_decay), jnp.zeros_like(local_total)),
    )
    from_device = running_decay + offsets[:, None, :]
    local_off = (
        jnp.einsum("blhn,bhpn->blhp", read_blocks, prefix, precision=HIGH)
        * jnp.exp(running_decay)[..., None]
    )
    far_off = (
        jnp.einsum("blhn,hpn->blhp", read_blocks, incoming, precision=HIGH)
        * jnp.exp(from_device)[..., None]
    )
    scan_out = (inner + local_off + far_off).reshape(length, local_heads, head_dim) + skip_scale[
        None, :, None
    ] * value_heads
    gated = scan_out.reshape(length, local_mix) * jax.nn.silu(gate_in.astype(jnp.float32))
    gate_squares = lax.psum(jnp.sum(gated * gated, axis=-1), "tp")
    state_out = (gated * lax.rsqrt(gate_squares / MIX_W + EPSILON)[:, None] * state_gain).astype(
        jnp.bfloat16
    )
    branch_rows = jnp.concatenate([pool_out, state_out], axis=1)
    out_weight = jnp.concatenate([out_pool_weight, out_state_weight], axis=0)
    terms = jnp.dot(
        branch_rows,
        lax.all_gather(out_weight, "sp", axis=1, tiled=True),
        preferred_element_type=jnp.float32,
    )
    result = lax.psum_scatter(terms, "tp", scatter_dimension=1, tiled=True)
    return result.astype(jnp.bfloat16)


def solution(mesh):
    placed = (
        P("sp", "tp"),
        P("tp"),
        P("sp", "tp"),
        P("sp", "tp"),
        P("sp", "tp"),
        P("sp", "tp"),
        P("sp", "tp"),
        P("sp", "tp"),
        P("tp", None, None),
        P("tp"),
        P(None, "tp"),
        P(None, "tp"),
        P(None, "tp"),
        P("tp"),
        P("tp"),
        P("sp", "tp"),
        P("tp"),
        P("tp"),
        P("tp", "sp"),
        P("tp", "sp"),
    )
    return jax.shard_map(
        local, mesh=mesh, in_specs=placed, out_specs=P("sp", "tp"), check_vma=False
    )
```

profile of v0, /device:TPU:0, one launch (start us, length us, event | category | flops | bytes accessed | tf_op | source)
XLA Modules:
  0.0 262.7 jit_solution(2948103364905407184)
XLA Ops:
  6.6 0.7 all-gather.7.cloned.1.call-update
  7.4 0.9 copy.40
  8.2 0.9 copy.41
  9.1 0.8 copy.42
  10.0 1.8 concatenate.21
  11.9 0.7 pad_maximum_fusion
  12.7 0.6 iota_compare_fusion
  13.3 6.2 %all-gather.1 = bf16[4,1,512]{2,1,0:T(2,128)(2,1)S(1)} all-gather(bf16[1,1,512]{2,1,0:T(2,128)(2,1)S(1)} %reshape.74), channel_id=1, replica_groups=mesh['sp'=8,'tp'=4] {'tp'}, dimensions={0}, use_global_device_ids=true | all-gather | bytes 5120 | tf_op jit(solution)/shard_map/all_gather | solution.py:80
  19.7 0.7 mul.207
  20.4 0.6 add_minimum_fusion
  21.0 13.2 %all-gather.7.cloned.1.call-done = bf16[512,2048]{1,0:T(8,128)(2,1)} async-done(((bf16[512,512]{1,0:T(8,128)(2,1)}), bf16[512,2048]{1,0:T(8,128)(2,1)}) %all-gather.7.cloned.1.call-update) | async-done | bytes 2097168 | tf_op jit(solution)/shard_map/all_gather | solution.py:79
  34.3 2.2 fusion.1
  36.5 72.7 %all-gather.9.cloned.1.call-done = bf16[2048,900]{1,0:T(8,128)(2,1)} async-done(((bf16[256,900]{1,0:T(8,128)(2,1)}), bf16[2048,900]{1,0:T(8,128)(2,1)}) %all-gather.9.cloned.1.call-update) | async-done | bytes 3686416 | tf_op jit(solution)/shard_map/all_gather | solution.py:77
  109.2 4.5 %fusion.57 = (bf16[512,900]{0,1:T(8,128)(2,1)S(1)}, f32[512,900]{0,1:T(8,128)S(1)}) fusion(bf16[2048,900]{1,0:T(8,128)(2,1)} %all-gather.9.cloned.1.call-done, bf16[512,2048]{1,0:T(8,128)(2,1)S(1)} %copy-done.1, f32[2048]{0:T(1024)S(1)} %bitcast.113, f32[512]{0:T(512)S(1)} %add_rsqrt_fusion.1), kind=kOutput, calls=%fused_computation.113 | convolution fusion | flops 1892091904 | bytes 8558592 | tf_op jit(solution)/shard_map/dot_general | solution.py:88
  113.9 2.5 collective-permute-start.1
  116.6 0.3 reduce_window_sum.24
  117.1 0.7 copy.48
  117.9 0.7 slice.139
  118.7 0.7 copy.52
  119.4 0.7 copy.57
  120.1 4.6 %collective-permute-start = (bf16[15,256]{0,1:T(8,128)(2,1)}, bf16[15,256]{0,1:T(8,128)(2,1)}, u32[]{:S(2)}, u32[]{:S(2)}) collective-permute-start(bf16[15,256]{0,1:T(8,128)(2,1)} %slice.139), channel_id=1, source_target_pairs={{0,4},{4,8},{8,12},{12,16},{16,20},{20,24},{24,28},{1,5},{5,9},{9,... | collective-permute-start | bytes 23048 | tf_op jit(solution)/shard_map/ppermute | solution.py:17
  124.7 16.9 %all-gather.2 = f32[8,1,4]{2,1,0:T(1,128)} all-gather(f32[1,1,4]{2,1,0:T(1,128)S(1)} %fusion.49), channel_id=1, replica_groups=mesh['sp'=8,'tp'=4] {'sp'}, dimensions={0}, use_global_device_ids=true | all-gather | bytes 144 | tf_op jit(solution)/shard_map/all_gather | solution.py:22
  141.6 0.2 maximum_convert_fusion
  141.8 0.9 multiply_convert_fusion
  143.1 0.6 copy-done.2
  143.7 0.9 fusion.32
  144.6 3.1 %while.26 = (s32[]{:T(128)}, f32[4,64,64]{2,1,0:T(8,128)S(1)}, f32[4,4,64,64]{3,2,1,0:T(8,128)}, f32[4,4]{1,0:T(4,128)S(1)}, f32[4,4,64,64]{3,2,1,0:T(8,128)S(1)}, /*index=5*/s32[]{:T(128)}, s32[]{:T(128)}) while((s32[]{:T(128)}, f32[4,64,64]{2,1,0:T(8,128)S(1)}, f32[4,4,64,64]{3,2,1,0:T(8,128)}, f32[4,4]{1,0:T(4,128)S(1)}, ...), condition=%wide.region_3.4_spmd.clone, body=%wide.region_2.3_spmd.clone.sunk | while | flops 65539 | bytes 393872 | solution.py:162
  144.7 0.7 bitcast_dynamic-update-slice_fusion.2
  145.4 0.7 bitcast_dynamic-update-slice_fusion.2
  146.2 0.7 bitcast_dynamic-update-slice_fusion.2
  147.0 0.7 bitcast_dynamic-update-slice_fusion.2
  147.8 34.8 %all-gather = f32[32,64,64]{2,1,0:T(8,128)S(1)} all-gather(f32[4,64,64]{2,1,0:T(8,128)S(1)} %get-tuple-element.78), channel_id=2, replica_groups=mesh['sp'=8,'tp'=4] {'sp'}, dimensions={0}, use_global_device_ids=true | all-gather | bytes 589824 | tf_op jit(solution)/shard_map/all_gather | solution.py:22
  182.8 1.3 fusion.12
  184.1 1.6 fusion.11
  185.7 2.9 %fusion.8 = f32[4,128,128,4]{2,1,3,0:T(8,128)S(1)} fusion(f32[4,128,4]{1,2,0:T(4,128)} %copy.48, pred[128,128]{1,0:T(8,128)(4,1)} %iota_compare_fusion, f32[4,128,64]{1,2,0:T(8,128)S(1)} %get-tuple-element.147, f32[4,128,64]{1,2,0:T(8,128)} %copy-done.2), kind=kOutput, calls=%fused_computation.19 | convolution fusion | flops 202113024 | bytes 1335296 | tf_op jit(solution)/shard_map/blhn,bshn->blsh/dot_general | solution.py:151
  188.7 2.2 fusion.10
  190.8 0.3 copy.58
  191.2 0.3 multiply_reduce_fusion
  191.5 5.7 %psum.7 = f32[512]{0:T(512)S(1)} all-reduce(f32[512]{0:T(512)S(1)} %get-tuple-element.132), channel_id=1, replica_groups=mesh['sp'=8,'tp'=4] {'tp'}, use_global_device_ids=true, to_apply=%region_8.9 | all-reduce | flops 512 | bytes 4096 | tf_op jit(solution)/shard_map/psum | solution.py:188
  197.3 1.0 maximum_convert_fusion.1
  198.3 0.2 slice_add_fusion.2
  198.5 0.2 slice_add_fusion.1
  198.8 0.2 slice_add_fusion
  199.2 0.3 slice_bitcast_fusion
  199.7 0.4 fusion.13
  200.1 4.8 %fusion.28 = f32[512,2048]{1,0:T(8,128)} fusion(bf16[512,2048]{1,0:T(8,128)(2,1)} %all-gather.11.cloned.1.call-done, bf16[512,256]{0,1:T(8,128)(2,1)S(1)} %multiply_convert_fusion.1, bf16[512,256]{0,1:T(8,128)(2,1)S(1)} %fusion.13), kind=kOutput, calls=%fused_computation.57 | convolution fusion | flops 1074790400 | bytes 6815744 | tf_op jit(solution)/shard_map/dot_general | solution.py:194
  205.0 49.1 %reduce-scatter.2.cloned.1.call-done = f32[512,512]{1,0:T(8,128)} async-done(((f32[512,2048]{1,0:T(8,128)}), f32[512,512]{1,0:T(8,128)}) %reduce-scatter.2.cloned.1.call-update) | async-done | bytes 1048592 | tf_op jit(solution)/shard_map/reduce_scatter | solution.py:199
  254.1 2.1 convert_element_type.70
  (81 shorter events, 2.4 us)
Async XLA Ops:
  6.5 193.0 %copy-start = (bf16[1,256,256]{2,1,0:T(8,128)(2,1)S(1)}, bf16[1,256,256]{2,1,0:T(8,128)(2,1)}, u32[]{:S(2)}) copy-start(bf16[1,256,256]{2,1,0:T(8,128)(2,1)} %param.32) | copy-start | bytes 393220
  6.5 5.3 %copy-start.4 = (bf16[256,256]{1,0:T(8,128)(2,1)S(1)}, bf16[256,256]{1,0:T(8,128)(2,1)}, u32[]{:S(2)}) copy-start(bf16[256,256]{1,0:T(8,128)(2,1)} %param.42) | copy-start | bytes 393220
  6.5 5.3 %copy-start.3 = (bf16[256,256]{1,0:T(8,128)(2,1)S(1)}, bf16[256,256]{1,0:T(8,128)(2,1)}, u32[]{:S(2)}) copy-start(bf16[256,256]{1,0:T(8,128)(2,1)} %param.43) | copy-start | bytes 393220
  6.5 6.8 %copy-start.12 = (bf16[512]{0:T(512)(128)(2,1)S(1)}, bf16[512]{0:T(512)(128)(2,1)}, u32[]{:S(2)}) copy-start(bf16[512]{0:T(512)(128)(2,1)} %param.25) | copy-start | bytes 3076
  6.5 12.9 %copy-start.6 = (f32[4,256]{1,0:T(4,128)S(1)}, f32[4,256]{1,0:T(4,128)}, u32[]{:S(2)}) copy-start(f32[4,256]{1,0:T(4,128)} %param.34) | copy-start | bytes 12292
  6.5 12.9 %copy-start.9 = (f32[4,64]{1,0:T(4,128)S(1)}, f32[4,64]{1,0:T(4,128)}, u32[]{:S(2)}) copy-start(f32[4,64]{1,0:T(4,128)} %param.35) | copy-start | bytes 3076
  6.6 12.9 %copy-start.8 = (f32[4,64]{1,0:T(4,128)S(1)}, f32[4,64]{1,0:T(4,128)}, u32[]{:S(2)}) copy-start(f32[4,64]{1,0:T(4,128)} %param.36) | copy-start | bytes 3076
  6.6 13.1 %copy-start.16 = (f32[4]{0:T(128)S(1)}, f32[4]{0:T(128)}, u32[]{:S(2)}) copy-start(f32[4]{0:T(128)} %param.38) | copy-start | bytes 52
  6.6 13.1 %copy-start.14 = (f32[4]{0:T(128)S(1)}, f32[4]{0:T(128)}, u32[]{:S(2)}) copy-start(f32[4]{0:T(128)} %param.40) | copy-start | bytes 52
  6.6 27.7 %all-gather.7.cloned.1.call-start = ((), (), s32[]{:S(2)}) async-start(), calls=%async_computation.1 | async-start | bytes 2621440 | tf_op jit(solution)/shard_map/all_gather | solution.py:79
  7.3 101.9 %all-gather.9.cloned.1.call-start = ((), (), s32[]{:S(2)}) async-start(), calls=%async_computation.2 | async-start | bytes 4718592 | tf_op jit(solution)/shard_map/all_gather | solution.py:77
  11.8 188.3 %all-gather.11.cloned.1.call-start = ((), (), s32[]{:S(2)}) async-start(), calls=%async_computation.3 | async-start | bytes 2359296 | tf_op jit(solution)/shard_map/all_gather | solution.py:196
  12.6 241.4 %reduce-scatter.2.cloned.1.call-start = ((), (), s32[]{:S(2)}) async-start(), calls=%async_computation.4 | async-start | bytes 5242880 | tf_op jit(solution)/shard_map/reduce_scatter | solution.py:199
  34.3 75.0 %copy-start.1 = (bf16[512,2048]{1,0:T(8,128)(2,1)S(1)}, bf16[512,2048]{1,0:T(8,128)(2,1)}, u32[]{:S(2)}) copy-start(bf16[512,2048]{1,0:T(8,128)(2,1)} %all-gather.7.cloned.1.call-done) | copy-start | bytes 6291460
  109.2 7.1 %copy-start.5 = (f32[512,4]{0,1:T(4,128)S(1)}, f32[512,4]{0,1:T(4,128)}, u32[]{:S(2)}) copy-start(f32[512,4]{0,1:T(4,128)} %param.39) | copy-start | bytes 24580
  109.2 7.1 %copy-start.13 = (f32[4]{0:T(128)S(1)}, f32[4]{0:T(128)}, u32[]{:S(2)}) copy-start(f32[4]{0:T(128)} %param.37) | copy-start | bytes 52
  113.9 27.7 %collective-permute-start.1 = (bf16[3,384]{0,1:T(8,128)(2,1)S(1)}, bf16[3,384]{0,1:T(8,128)(2,1)S(1)}, u32[]{:S(2)}, u32[]{:S(2)}) collective-permute-start(bf16[3,384]{0,1:T(8,128)(2,1)S(1)} %slice.152), channel_id=1, source_target_pairs={{0,4},{4,8},{8,12},{12,16},{16,20},{20,24},{24,28},{1,5},{5,9},{9,... | collective-permute-start | bytes 6920 | tf_op jit(solution)/shard_map/ppermute | solution.py:17
  120.1 77.1 %collective-permute-start = (bf16[15,256]{0,1:T(8,128)(2,1)}, bf16[15,256]{0,1:T(8,128)(2,1)}, u32[]{:S(2)}, u32[]{:S(2)}) collective-permute-start(bf16[15,256]{0,1:T(8,128)(2,1)} %slice.139), channel_id=1, source_target_pairs={{0,4},{4,8},{8,12},{12,16},{16,20},{20,24},{24,28},{1,5},{5,9},{9,... | collective-permute-start | bytes 23048 | tf_op jit(solution)/shard_map/ppermute | solution.py:17
  143.0 0.7 copy-start.2
  188.6 2.5 copy-start.7
  190.8 6.3 %copy-start.11 = (f32[256]{0:T(256)S(1)}, f32[256]{0:T(256)}, u32[]{:S(2)}) copy-start(f32[256]{0:T(256)} %param.41) | copy-start | bytes 3076
  199.0 0.7 copy-start.10
  199.0 0.7 copy-start.15
Sparse Core Ops, SparseCore 0:
  9.0 25.2 all-gather.6
  36.4 72.7 all-gather.8
  111.3 60.4 all-gather.10
  205.1 48.9 reduce-scatter.1
where the time goes:
time: 263 us
  waiting for transfers between devices  136 us (52%)
  blocking collectives  63.5 us (24%)
  matrix products  18.7 us (7%)
  between operations  13.6 us (5%)
  other arithmetic  13.4 us (5%)
  local copies, waits for them, and re-layouts  10.1 us (4%)
  starting transfers between devices  7.23 us (3%)
    all_gather x1, waiting for transfers between devices, local(): in_weight = lax.all_gather(joined, 'sp', axis=0, tiled=True)  72.7 us
    all_gather x2, blocking collectives, carried_in(): gathered = jax.tree.map(lambda a: lax.all_gather(a, axis), part)  51.7 us
    reduce_scatter x1, waiting for transfers between devices, local(): result = lax.psum_scatter(terms, 'tp', scatter_dimension=1, tiled=True)  49.1 us
    all_gather x1, waiting for transfers between devices, local(): lax.all_gather(activations, 'tp', axis=1, tiled=True)  13.2 us
    ppermute x2, starting transfers between devices, shifted(): lax.ppermute(value, axis, [(source, source + steps) for source in range(l...  7.07 us
    all_gather x1, blocking collectives, local(): lax.all_gather(norm_gain, 'tp', axis=0, tiled=True)  6.15 us
    psum x1, blocking collectives, local(): gate_squares = lax.psum(jnp.sum(gated * gated, axis=-1), 'tp')  5.66 us
  transfers between devices with their start and end apart: 6, of which 3 were waited for; matrix products, arithmetic and copies ran while one was open for 13% of the time, Pallas kernels for 0%

commit v1 on v0

--- a/solution.py
+++ b/solution.py
@@ -75,10 +75,12 @@
         [pool_weight, gate_weight, value_weight, key_weight, read_weight, step_weight], axis=1
     )
     in_weight = lax.all_gather(joined, "sp", axis=0, tiled=True)
-    whole, gains = (
-        lax.all_gather(activations, "tp", axis=1, tiled=True),
-        lax.all_gather(norm_gain, "tp", axis=0, tiled=True),
-    )
+
+    def end_spans(packet):
+        f_next = lax.all_to_all(jnp.stack([packet for _ in range(lax.axis_size("tp"))]), "tp", 0, 0)
+        return jnp.concatenate(f_next, axis=1)
+
+    whole, gains = (end_spans(activations), lax.all_gather(norm_gain, "tp", axis=0, tiled=True))
     widened_rows = whole.astype(jnp.float32)
     normed = (
         widened_rows

time: 263 us -> 240 us (0.913)
  waiting for transfers between devices: 136 us -> 86.4 us
  blocking collectives: 63.5 us -> 83.6 us
  starting transfers between devices: 7.23 us -> 11.5 us
    all_gather x1, waiting for transfers between devices: 72.7 us -> 37.6 us  [local(): in_weight = lax.all_gather(joined, 'sp', axis=0, tiled=True)]
    all_gather x1, blocking collectives: 6.15 us -> 25.8 us  [local(): lax.all_gather(norm_gain, 'tp', axis=0, tiled=True)]
    all_gather x1 -> x0, waiting for transfers between devices: 13.2 us -> none  [local(): lax.all_gather(activations, 'tp', axis=1, tiled=True)]
    all_to_all x0 -> x1, starting transfers between devices: none -> 4.38 us  [end_spans(): lax.all_to_all(jnp.stack([packet for _ in range(lax.axis_size('tp'))]), '...]
  transfers between devices with their start and end apart: 6 -> 6, of which waited for: 3 -> 2; matrix products, arithmetic and copies ran while one was open for 13% -> 13% of each run, Pallas kernels for 0% -> 0%
where the time goes in v1:
time: 240 us; the launch traced here: 239 us
  waiting for transfers between devices  86.4 us (36%)
  blocking collectives  83.6 us (35%)
  matrix products  18.1 us (8%)
  between operations  13.7 us (6%)
  other arithmetic  13.6 us (6%)
  local copies, waits for them, and re-layouts  11.9 us (5%)
  starting transfers between devices  11.5 us (5%)
    all_gather x2, blocking collectives, carried_in(): gathered = jax.tree.map(lambda a: lax.all_gather(a, axis), part)  52.2 us
    reduce_scatter x1, waiting for transfers between devices, local(): result = lax.psum_scatter(terms, 'tp', scatter_dimension=1, tiled=True)  48.6 us
    all_gather x1, waiting for transfers between devices, local(): in_weight = lax.all_gather(joined, 'sp', axis=0, tiled=True)  37.6 us
    all_gather x1, blocking collectives, local(): lax.all_gather(norm_gain, 'tp', axis=0, tiled=True)  25.8 us
    ppermute x2, starting transfers between devices, shifted(): lax.ppermute(value, axis, [(source, source + steps) for source in range(l...  7.08 us
    psum x1, blocking collectives, local(): gate_squares = lax.psum(jnp.sum(gated * gated, axis=-1), 'tp')  5.66 us
    dot_general x1, matrix products, local(): projected = jnp.dot(normed, in_weight, preferred_element_type=jnp.float32)  4.98 us
    dot_general x1, matrix products, local(): jnp.dot(branch_rows, lax.all_gather(out_weight, 'sp', axis=1, tiled=True)...  4.84 us
  transfers between devices with their start and end apart: 6, of which 2 were waited for; matrix products, arithmetic and copies ran while one was open for 13% of the time, Pallas kernels for 0%

profile of v1, /device:TPU:0, one launch (start us, length us, event | category | flops | bytes accessed | tf_op | source)
XLA Modules:
  0.0 239.0 jit_solution(13504134465375346958)
XLA Ops:
  6.5 0.9 copy.61
  7.5 0.9 copy.62
  8.4 0.8 copy.63
  9.2 1.8 concatenate.21
  11.2 1.5 stack.22
  12.8 4.4 %all-to-all-start = ((bf16[4,512,512]{1,2,0:T(8,128)(2,1)}), bf16[4,512,512]{1,2,0:T(8,128)(2,1)S(1)}, u32[]{:S(2)}, u32[]{:S(2)}) async-start(bf16[4,512,512]{1,2,0:T(8,128)(2,1)} %stack.22), calls=%async_computation | async-start | bytes 4194304 | tf_op jit(solution)/shard_map/all_to_all | solution.py:80
  17.2 0.7 pad_maximum_fusion
  18.1 25.8 %all-gather.1 = bf16[4,1,512]{2,1,0:T(2,128)(2,1)S(1)} all-gather(bf16[1,1,512]{2,1,0:T(2,128)(2,1)S(1)} %reshape.81), channel_id=1, replica_groups=mesh['sp'=8,'tp'=4] {'tp'}, dimensions={0}, use_global_device_ids=true | all-gather | bytes 5120 | tf_op jit(solution)/shard_map/all_gather | solution.py:83
  44.0 0.7 mul.209
  44.7 0.6 add_minimum_fusion
  45.4 0.6 iota_compare_fusion
  46.0 0.6 slice_reduce_fusion.3
  46.6 0.5 multiply_reduce_fusion
  47.1 1.9 fusion.2
  49.0 37.6 %all-gather.6.cloned.1.call-done = bf16[2048,900]{1,0:T(8,128)(2,1)} async-done(((bf16[256,900]{1,0:T(8,128)(2,1)}), bf16[2048,900]{1,0:T(8,128)(2,1)}) %all-gather.6.cloned.1.call-update) | async-done | bytes 3686416 | tf_op jit(solution)/shard_map/all_gather | solution.py:77
  86.7 5.0 %fusion.52 = (bf16[512,900]{0,1:T(8,128)(2,1)S(1)}, f32[512,900]{0,1:T(8,128)S(1)}) fusion(bf16[512,2048]{0,1:T(8,128)(2,1)} %fusion.2, bf16[2048,900]{1,0:T(8,128)(2,1)} %all-gather.6.cloned.1.call-done), kind=kOutput, calls=%fused_computation.109 | convolution fusion | flops 1887897600 | bytes 8548352 | tf_op jit(solution)/shard_map/dot_general | solution.py:90
  91.8 2.5 %collective-permute-start.1 = (bf16[3,384]{0,1:T(8,128)(2,1)S(1)}, bf16[3,384]{0,1:T(8,128)(2,1)S(1)}, u32[]{:S(2)}, u32[]{:S(2)}) collective-permute-start(bf16[3,384]{0,1:T(8,128)(2,1)S(1)} %slice.152), channel_id=1, source_target_pairs={{0,4},{4,8},{8,12},{12,16},{16,20},{20,24},{24,28},{1,5},{5,9},{9,... | collective-permute-start | bytes 6920 | tf_op jit(solution)/shard_map/ppermute | solution.py:17
  94.5 0.3 reduce_window_sum.24
  95.1 0.7 copy.69
  95.8 0.7 slice.139
  96.6 0.7 copy.73
  97.3 0.7 copy.77
  98.0 4.6 %collective-permute-start = (bf16[15,256]{0,1:T(8,128)(2,1)}, bf16[15,256]{0,1:T(8,128)(2,1)}, u32[]{:S(2)}, u32[]{:S(2)}) collective-permute-start(bf16[15,256]{0,1:T(8,128)(2,1)} %slice.139), channel_id=1, source_target_pairs={{0,4},{4,8},{8,12},{12,16},{16,20},{20,24},{24,28},{1,5},{5,9},{9,... | collective-permute-start | bytes 23048 | tf_op jit(solution)/shard_map/ppermute | solution.py:17
  102.6 17.2 %all-gather.2 = f32[8,1,4]{2,1,0:T(1,128)} all-gather(f32[1,1,4]{2,1,0:T(1,128)S(1)} %fusion.44), channel_id=1, replica_groups=mesh['sp'=8,'tp'=4] {'sp'}, dimensions={0}, use_global_device_ids=true | all-gather | bytes 144 | tf_op jit(solution)/shard_map/all_gather | solution.py:22
  120.1 0.9 multiply_convert_fusion
  121.4 0.9 fusion.27
  122.3 3.1 %while.26 = (s32[]{:T(128)}, f32[4,64,64]{2,1,0:T(8,128)S(1)}, f32[4,4,64,64]{3,2,1,0:T(8,128)}, f32[4,4]{1,0:T(4,128)S(1)}, f32[4,4,64,64]{3,2,1,0:T(8,128)S(1)}, /*index=5*/s32[]{:T(128)}, s32[]{:T(128)}) while((s32[]{:T(128)}, f32[4,64,64]{2,1,0:T(8,128)S(1)}, f32[4,4,64,64]{3,2,1,0:T(8,128)}, f32[4,4]{1,0:T(4,128)S(1)}, ...), condition=%wide.region_3.4_spmd.clone, body=%wide.region_2.3_spmd.clone.sunk | while | flops 65539 | bytes 393872 | solution.py:164
  122.4 0.7 bitcast_dynamic-update-slice_fusion.2
  123.1 0.7 bitcast_dynamic-update-slice_fusion.2
  123.9 0.7 bitcast_dynamic-update-slice_fusion.2
  124.7 0.7 bitcast_dynamic-update-slice_fusion.2
  125.4 35.0 %all-gather = f32[32,64,64]{2,1,0:T(8,128)S(1)} all-gather(f32[4,64,64]{2,1,0:T(8,128)S(1)} %get-tuple-element.78), channel_id=2, replica_groups=mesh['sp'=8,'tp'=4] {'sp'}, dimensions={0}, use_global_device_ids=true | all-gather | bytes 589824 | tf_op jit(solution)/shard_map/all_gather | solution.py:22
  160.6 1.3 fusion.7
  161.9 1.6 fusion.6
  163.5 2.9 %fusion.3 = f32[4,128,128,4]{1,2,3,0:T(8,128)S(1)} fusion(f32[4,128,4]{1,2,0:T(4,128)} %copy.69, pred[128,128]{0,1:T(8,128)(4,1)} %iota_compare_fusion, f32[4,128,64]{1,2,0:T(8,128)S(1)} %get-tuple-element.152, f32[4,128,64]{1,2,0:T(8,128)} %copy-done.2), kind=kOutput, calls=%fused_computation.15 | convolution fusion | flops 202113024 | bytes 1335296 | tf_op jit(solution)/shard_map/blhn,bshn->blsh/dot_general | solution.py:153
  166.5 1.1 fusion.5
  167.6 0.3 copy.78
  167.9 0.3 multiply_reduce_fusion.1
  168.2 5.7 %psum.7 = f32[512]{0:T(512)S(1)} all-reduce(f32[512]{0:T(512)S(1)} %get-tuple-element.137), channel_id=1, replica_groups=mesh['sp'=8,'tp'=4] {'tp'}, use_global_device_ids=true, to_apply=%region_8.9 | all-reduce | flops 512 | bytes 4096 | tf_op jit(solution)/shard_map/psum | solution.py:190
  174.0 1.0 maximum_convert_fusion.1
  175.0 0.2 slice_add_fusion.2
  175.3 0.2 slice_add_fusion.1
  175.5 0.2 slice_add_fusion
  176.0 0.3 slice_bitcast_fusion
  176.4 0.4 fusion.8
  176.9 4.8 %fusion.23 = f32[512,2048]{1,0:T(8,128)} fusion(bf16[512,2048]{1,0:T(8,128)(2,1)} %all-gather.8.cloned.1.call-done, bf16[512,256]{0,1:T(8,128)(2,1)S(1)} %multiply_convert_fusion.1, bf16[512,256]{0,1:T(8,128)(2,1)S(1)} %fusion.8), kind=kOutput, calls=%fused_computation.53 | convolution fusion | flops 1074790400 | bytes 6815744 | tf_op jit(solution)/shard_map/dot_general | solution.py:196
  181.7 48.6 %reduce-scatter.2.cloned.1.call-done = f32[512,512]{1,0:T(8,128)} async-done(((f32[512,2048]{1,0:T(8,128)}), f32[512,512]{1,0:T(8,128)}) %reduce-scatter.2.cloned.1.call-update) | async-done | bytes 1048592 | tf_op jit(solution)/shard_map/reduce_scatter | solution.py:201
  230.4 2.1 convert_element_type.83
  (91 shorter events, 2.7 us)
Async XLA Ops:
  6.5 169.8 %copy-start = (bf16[1,256,256]{2,1,0:T(8,128)(2,1)S(1)}, bf16[1,256,256]{2,1,0:T(8,128)(2,1)}, u32[]{:S(2)}) copy-start(bf16[1,256,256]{2,1,0:T(8,128)(2,1)} %param.32) | copy-start | bytes 393220
  6.5 4.5 %copy-start.1 = (bf16[512,512]{1,0:T(8,128)(2,1)S(1)}, bf16[512,512]{1,0:T(8,128)(2,1)}, u32[]{:S(2)}) copy-start(bf16[512,512]{1,0:T(8,128)(2,1)} %param.24) | copy-start | bytes 1572868
  6.5 80.2 %all-gather.6.cloned.1.call-start = ((), (), s32[]{:S(2)}) async-start(), calls=%async_computation.2 | async-start | bytes 4718592 | tf_op jit(solution)/shard_map/all_gather | solution.py:77
  12.8 4.4 %copy-start.3 = (bf16[256,256]{1,0:T(8,128)(2,1)S(1)}, bf16[256,256]{1,0:T(8,128)(2,1)}, u32[]{:S(2)}) copy-start(bf16[256,256]{1,0:T(8,128)(2,1)} %param.43) | copy-start | bytes 393220
  12.8 4.4 %copy-start.4 = (bf16[256,256]{1,0:T(8,128)(2,1)S(1)}, bf16[256,256]{1,0:T(8,128)(2,1)}, u32[]{:S(2)}) copy-start(bf16[256,256]{1,0:T(8,128)(2,1)} %param.42) | copy-start | bytes 393220
  12.8 5.3 %copy-start.16 = (bf16[512]{0:T(512)(128)(2,1)S(1)}, bf16[512]{0:T(512)(128)(2,1)}, u32[]{:S(2)}) copy-start(bf16[512]{0:T(512)(128)(2,1)} %param.25) | copy-start | bytes 3076
  12.8 31.1 %copy-start.18 = (f32[4]{0:T(128)S(1)}, f32[4]{0:T(128)}, u32[]{:S(2)}) copy-start(f32[4]{0:T(128)} %param.40) | copy-start | bytes 52
  12.8 32.5 %copy-start.10 = (f32[4,256]{1,0:T(4,128)S(1)}, f32[4,256]{1,0:T(4,128)}, u32[]{:S(2)}) copy-start(f32[4,256]{1,0:T(4,128)} %param.34) | copy-start | bytes 12292
  12.8 32.5 %copy-start.12 = (f32[4,64]{1,0:T(4,128)S(1)}, f32[4,64]{1,0:T(4,128)}, u32[]{:S(2)}) copy-start(f32[4,64]{1,0:T(4,128)} %param.36) | copy-start | bytes 3076
  12.8 32.5 %copy-start.13 = (f32[4,64]{1,0:T(4,128)S(1)}, f32[4,64]{1,0:T(4,128)}, u32[]{:S(2)}) copy-start(f32[4,64]{1,0:T(4,128)} %param.35) | copy-start | bytes 3076
  12.8 33.8 %copy-start.20 = (f32[4]{0:T(128)S(1)}, f32[4]{0:T(128)}, u32[]{:S(2)}) copy-start(f32[4]{0:T(128)} %param.38) | copy-start | bytes 52
  12.8 33.8 %all-to-all-start = ((bf16[4,512,512]{1,2,0:T(8,128)(2,1)}), bf16[4,512,512]{1,2,0:T(8,128)(2,1)S(1)}, u32[]{:S(2)}, u32[]{:S(2)}) async-start(bf16[4,512,512]{1,2,0:T(8,128)(2,1)} %stack.22), calls=%async_computation | async-start | bytes 4194304 | tf_op jit(solution)/shard_map/all_to_all | solution.py:80
  17.2 159.7 %all-gather.8.cloned.1.call-start = ((), (), s32[]{:S(2)}) async-start(), calls=%async_computation.3 | async-start | bytes 2359296 | tf_op jit(solution)/shard_map/all_gather | solution.py:198
  18.0 212.4 %reduce-scatter.2.cloned.1.call-start = ((), (), s32[]{:S(2)}) async-start(), calls=%async_computation.4 | async-start | bytes 5242880 | tf_op jit(solution)/shard_map/reduce_scatter | solution.py:201
  49.0 45.2 %copy-start.9 = (f32[512,4]{0,1:T(4,128)S(1)}, f32[512,4]{0,1:T(4,128)}, u32[]{:S(2)}) copy-start(f32[512,4]{0,1:T(4,128)} %param.39) | copy-start | bytes 24580
  49.0 45.2 %copy-start.17 = (f32[4]{0:T(128)S(1)}, f32[4]{0:T(128)}, u32[]{:S(2)}) copy-start(f32[4]{0:T(128)} %param.37) | copy-start | bytes 52
  91.8 28.1 %collective-permute-start.1 = (bf16[3,384]{0,1:T(8,128)(2,1)S(1)}, bf16[3,384]{0,1:T(8,128)(2,1)S(1)}, u32[]{:S(2)}, u32[]{:S(2)}) collective-permute-start(bf16[3,384]{0,1:T(8,128)(2,1)S(1)} %slice.152), channel_id=1, source_target_pairs={{0,4},{4,8},{8,12},{12,16},{16,20},{20,24},{24,28},{1,5},{5,9},{9,... | collective-permute-start | bytes 6920 | tf_op jit(solution)/shard_map/ppermute | solution.py:17
  95.0 25.1 %copy-start.5 = (f32[384]{0:T(512)S(1)}, f32[384]{0:T(512)}, u32[]{:S(2)}) copy-start(f32[384]{0:T(512)} %get-tuple-element.113) | copy-start | bytes 4612
  95.0 25.1 %copy-start.6 = (f32[384]{0:T(512)S(1)}, f32[384]{0:T(512)}, u32[]{:S(2)}) copy-start(f32[384]{0:T(512)} %get-tuple-element.114) | copy-start | bytes 4612
  95.0 25.1 %copy-start.7 = (f32[384]{0:T(512)S(1)}, f32[384]{0:T(512)}, u32[]{:S(2)}) copy-start(f32[384]{0:T(512)} %get-tuple-element.115) | copy-start | bytes 4612
  95.0 25.1 %copy-start.8 = (f32[384]{0:T(512)S(1)}, f32[384]{0:T(512)}, u32[]{:S(2)}) copy-start(f32[384]{0:T(512)} %get-tuple-element.116) | copy-start | bytes 4612
  98.0 76.0 %collective-permute-start = (bf16[15,256]{0,1:T(8,128)(2,1)}, bf16[15,256]{0,1:T(8,128)(2,1)}, u32[]{:S(2)}, u32[]{:S(2)}) collective-permute-start(bf16[15,256]{0,1:T(8,128)(2,1)} %slice.139), channel_id=1, source_target_pairs={{0,4},{4,8},{8,12},{12,16},{16,20},{20,24},{24,28},{1,5},{5,9},{9,... | collective-permute-start | bytes 23048 | tf_op jit(solution)/shard_map/ppermute | solution.py:17
  121.4 1.0 copy-start.2
  166.5 1.5 copy-start.11
  167.6 6.3 %copy-start.15 = (f32[256]{0:T(256)S(1)}, f32[256]{0:T(256)}, u32[]{:S(2)}) copy-start(f32[256]{0:T(256)} %param.41) | copy-start | bytes 3076
  175.8 0.7 copy-start.14
  175.8 0.7 copy-start.19
Sparse Core Ops, SparseCore 0:
  11.1 75.5 all-gather.5
  88.7 60.9 all-gather.7
  181.9 48.4 reduce-scatter.1
